TPU v7x, 256 devices: a 4x2x16 block of a 4x16x16 slice. The times are simulated.
256 devices in a mesh: grp: 2 (over y), ep: 64 (over z, x), tp: 2 (over core).
Axes of the slice: x: 4, y: 2, z: 16, core: 2. Of those that a mesh axis runs over, the one named last changes fastest.
The devices are a block of a 4x16x16 slice.
Arguments:
- tokens: bfloat16 [12288, 2048], P(('grp', 'ep')), parts along dimension 0, may hold values from -6 to 6
- prior_state: float32 [2, 12288, 4096], P(None, ('grp', 'ep'), 'tp'), parts along dimension 1, may hold values from -6 to 6
- mix_gain: float32 [2048], replicated, may hold values from 0.1 to 1.9
- in_weight: bfloat16 [2048, 1024], P(None, 'tp'), may hold values from -0.125 to 0.125
- decay_rate: float32 [64, 64], P('tp'), may hold values from 0.2 to 20
- frequency: float32 [64, 64], P('tp'), may hold values from 0 to 12
- log_step: float32 [64], P('tp'), may hold values from -4.6 to 0
- input_map: float32 [2, 64, 64, 16], P(None, 'tp'), may hold values from -6 to 6
- output_map: float32 [2, 64, 16, 64], P(None, 'tp'), may hold values from -0.5 to 0.5
- skip_gain: float32 [1024], P('tp'), may hold values from -4 to 4
- out_weight: bfloat16 [1024, 2048], P('tp'), may hold values from -0.1875 to 0.1875
- channel_gain: float32 [2048], replicated, may hold values from 0.1 to 1.9
- expert_gate: bfloat16 [64, 2048, 512], P('ep', None, 'tp'), may hold values from -0.125 to 0.125
- expert_up: bfloat16 [64, 2048, 512], P('ep', None, 'tp'), may hold values from -0.125 to 0.125
- expert_down: bfloat16 [64, 512, 2048], P('ep', 'tp'), may hold values from -0.25 to 0.25
- shared_gate: bfloat16 [2048, 512], P(None, 'tp'), may hold values from -0.125 to 0.125
- shared_up: bfloat16 [2048, 512], P(None, 'tp'), may hold values from -0.125 to 0.125
- shared_down: bfloat16 [512, 2048], P('tp'), may hold values from -0.25 to 0.25
- routes: int32 [12288, 6], P(('grp', 'ep')), parts along dimension 0, may hold values from 0 to 63, all different within a row; in each aligned block of 96 rows (0 to 95, 96 to 191, ...) at most 13 rows name the same one
- route_weights: float32 [12288, 6], P(('grp', 'ep')), parts along dimension 0, may hold values from 0.05 to 0.8
Outputs:
- layer_out: bfloat16 [12288, 2048], P(('grp', 'ep'), 'tp'), parts along dimension 0
- new_state: float32 [2, 12288, 4096], P(None, ('grp', 'ep'), 'tp'), parts along dimension 1
There are 2 independent parts, one for each index of `grp`. A program takes and returns all parts, laid end to end along the dimension named above; an argument that names none is the same for every part. Nothing has to cross between parts.
Inputs may be any that keep to these rules, and one draw needn't show every extreme that they name: `routes`: each row names 6 different experts; among the rows of one index of ep no expert is named by more than 13 rows.
All inputs are finite; a program needn't handle non-finite values.
Results may differ from a plain program's by a relative error of at most 0.017.
Values may be sent and summed in bfloat16 or wider, within the bound.
No kernel may reach another device: no remote copies, remote signals or barrier semaphores. Data moves between devices by JAX's collectives and lax.ppermute only.
A program may use at most 128 MiB of HBM per device.

v0:
```python
import jax
import jax.numpy as jnp
from jax import lax
from jax.sharding import PartitionSpec as P

norm_eps = 1e-06


def copy_for_each(value, axis):
    peers = lax.axis_size(axis)
    return lax.all_to_all(
        jnp.broadcast_to(value[None], (peers, *value.shape)), axis, 0, 0, tiled=True
    )


def of_everyone(value, axis):
    return copy_for_each(value, axis).astype(jnp.float32).sum(axis=0)


def in_blocks(value, dim, peers):
    before, after = (value.shape[:dim], value.shape[dim + 1 :])
    return jnp.moveaxis(value.reshape(*before, peers, -1, *after), dim, 0)


def summed_on_arrival(value, axis, dim):
    tiles = in_blocks(value, dim, lax.axis_size(axis))
    arrived = lax.all_to_all(tiles, axis, split_axis=0, concat_axis=0, tiled=True)
    return arrived.astype(jnp.float32).sum(axis=0)


def root_scale(activations, scale_gain):
    values = activations.astype(jnp.float32)
    factor = lax.rsqrt(jnp.mean(values * values, axis=-1, keepdims=True) + norm_eps)
    return (values * factor * scale_gain).astype(jnp.bfloat16)


def state_update(
    drive_rows, prior_state, decay_rate, frequency, log_step, input_map, output_map, skip_gain
):
    sequences = drive_rows.shape[0]
    groups = decay_rate.shape[0]
    driven = drive_rows.astype(jnp.float32).reshape(sequences, groups, -1)
    step_size = jnp.exp(log_step)[:, None]
    real_rate = -decay_rate
    magnitude = jnp.exp(real_rate * step_size)
    turn_real = magnitude * jnp.cos(frequency * step_size)
    turn_imag = magnitude * jnp.sin(frequency * step_size)
    denominator = real_rate * real_rate + frequency * frequency
    hold_real = ((turn_real - 1.0) * real_rate + turn_imag * frequency) / denominator
    hold_imag = (turn_imag * real_rate - (turn_real - 1.0) * frequency) / denominator
    push_real = jnp.einsum("sgh,gph->sgp", driven, input_map[0])
    push_imag = jnp.einsum("sgh,gph->sgp", driven, input_map[1])
    enter_real = push_real * hold_real - push_imag * hold_imag
    enter_imag = push_real * hold_imag + push_imag * hold_real
    old_real = prior_state[0].reshape(sequences, groups, -1)
    old_imag = prior_state[1].reshape(sequences, groups, -1)
    fresh_real = turn_real * old_real - turn_imag * old_imag + enter_real
    fresh_imag = turn_real * old_imag + turn_imag * old_real + enter_imag
    readout = jnp.einsum("ghp,sgp->sgh", output_map[0], fresh_real)
    readout = readout - jnp.einsum("ghp,sgp->sgh", output_map[1], fresh_imag)
    readout = readout.reshape(sequences, -1) + skip_gain * drive_rows.astype(jnp.float32)
    fresh = jnp.stack([fresh_real.reshape(sequences, -1), fresh_imag.reshape(sequences, -1)])
    return (readout, fresh)


def body(
    tokens,
    prior_state,
    mix_gain,
    in_weight,
    decay_rate,
    frequency,
    log_step,
    input_map,
    output_map,
    skip_gain,
    out_weight,
    channel_gain,
    expert_gate,
    expert_up,
    expert_down,
    shared_gate,
    shared_up,
    shared_down,
    routes,
    route_weights,
):
    normed = root_scale(tokens, mix_gain)
    drive_rows = jnp.dot(normed, in_weight, preferred_element_type=jnp.float32).astype(jnp.bfloat16)
    readout, new_state = state_update(
        drive_rows, prior_state, decay_rate, frequency, log_step, input_map, output_map, skip_gain
    )
    activated = jax.nn.gelu(readout).astype(jnp.bfloat16)
    partial_value = jnp.dot(activated, out_weight, preferred_element_type=jnp.float32)
    mixer_out = of_everyone(partial_value.astype(jnp.bfloat16), "tp").astype(jnp.float32)
    middle = (tokens.astype(jnp.float32) + mixer_out).astype(jnp.bfloat16)
    second_normed = root_scale(middle, channel_gain)
    shared_gval = jnp.dot(second_normed, shared_gate, preferred_element_type=jnp.float32)
    shared_uval = jnp.dot(second_normed, shared_up, preferred_element_type=jnp.float32)
    shared_hidden = (jax.nn.silu(shared_gval) * shared_uval).astype(jnp.bfloat16)
    shared_piece = jnp.dot(shared_hidden, shared_down, preferred_element_type=jnp.float32)
    shared_out = summed_on_arrival(shared_piece.astype(jnp.bfloat16), "tp", 1)
    experts = lax.axis_size("ep")
    seq_rows, top_count = routes.shape
    slot_cap = min(seq_rows, max(2, 3 * seq_rows * top_count // (2 * experts)))
    flat_routes = routes.reshape(-1)
    one_hot = (flat_routes[:, None] == jnp.arange(experts, dtype=jnp.int32)[None, :]).astype(
        jnp.int32
    )
    ranked = jnp.sum((jnp.cumsum(one_hot, axis=0) - one_hot) * one_hot, axis=1)
    slot_index = flat_routes * slot_cap + ranked
    placed = slot_index[:, None] == jnp.arange(experts * slot_cap, dtype=jnp.int32)[None, :]
    placed_rows = jnp.any(placed.reshape(seq_rows, top_count, experts * slot_cap), axis=1).astype(
        jnp.bfloat16
    )
    outgoing = lax.dot_general(
        placed_rows, second_normed, (((0,), (0,)), ((), ())), preferred_element_type=jnp.float32
    ).astype(jnp.bfloat16)
    outgoing = outgoing.reshape(experts, slot_cap, -1)
    half_cols = outgoing.shape[2] // lax.axis_size("tp")
    own_cols = lax.dynamic_slice_in_dim(outgoing, lax.axis_index("tp") * half_cols, half_cols, 2)
    arrived = lax.all_gather(
        lax.all_to_all(own_cols, "ep", split_axis=0, concat_axis=0, tiled=True),
        "tp",
        axis=2,
        tiled=True,
    )
    sources, count_items, full_width = arrived.shape
    expert_rows = arrived.reshape(sources * count_items, full_width)
    gate_val = jnp.dot(expert_rows, expert_gate[0], preferred_element_type=jnp.float32)
    up_val = jnp.dot(expert_rows, expert_up[0], preferred_element_type=jnp.float32)
    hidden = (jax.nn.silu(gate_val) * up_val).astype(jnp.bfloat16)
    piece = jnp.dot(hidden, expert_down[0], preferred_element_type=jnp.float32)
    summed = summed_on_arrival(
        piece.reshape(sources, count_items, full_width).astype(jnp.bfloat16), "tp", 2
    )
    returned = lax.all_to_all(
        summed.astype(jnp.bfloat16), "ep", split_axis=0, concat_axis=0, tiled=True
    )
    flat_back = returned.reshape(experts * slot_cap, -1)
    picked = (
        jnp.take(flat_back, slot_index, axis=0).reshape(seq_rows, top_count, -1).astype(jnp.float32)
    )
    routed = jnp.einsum("sk,skd->sd", route_weights, picked)
    own_middle = lax.dynamic_slice_in_dim(middle, lax.axis_index("tp") * half_cols, half_cols, 1)
    layer_out = (own_middle.astype(jnp.float32) + routed + shared_out).astype(jnp.bfloat16)
    return (layer_out, new_state)


def solution(mesh):
    in_specs = (
        P(("grp", "ep"), None),
        P(None, ("grp", "ep"), "tp"),
        P(),
        P(None, "tp"),
        P("tp", None),
        P("tp", None),
        P("tp"),
        P(None, "tp", None, None),
        P(None, "tp", None, None),
        P("tp"),
        P("tp", None),
        P(),
        P("ep", None, "tp"),
        P("ep", None, "tp"),
        P("ep", "tp", None),
        P(None, "tp"),
        P(None, "tp"),
        P("tp", None),
        P(("grp", "ep"), None),
        P(("grp", "ep"), None),
    )
    out_specs = (P(("grp", "ep"), "tp"), P(None, ("grp", "ep"), "tp"))
    return jax.shard_map(body, mesh=mesh, in_specs=in_specs, out_specs=out_specs, check_vma=False)
```

profile of v0, /device:TPU:34, one launch (start us, length us, event | category | flops | bytes accessed | tf_op | source)
XLA Modules:
  0.0 344.4 jit_solution(5603154047995699530)
XLA Ops:
  9.2 2.3 convolution_convert_fusion.4
  11.6 2.7 fusion.72
  15.8 2.5 copy.90
  19.8 3.0 bitcast_add_fusion
  25.8 3.7 %all-to-all-start = ((bf16[2,96,2048]{2,1,0:T(8,128)(2,1)}), bf16[2,96,2048]{2,1,0:T(8,128)(2,1)S(1)}, u32[]{:S(2)}, u32[]{:S(2)}) async-start(bf16[2,96,2048]{2,1,0:T(8,128)(2,1)} %broadcast_in_dim.9), calls=%async_computation | async-start | bytes 1572864 | tf_op jit(solution)/shard_map/all_to_all | solution.py:11
  34.7 2.9 reshape.128
  37.6 1.8 constant_dynamic-slice_fusion
  39.4 128.1 %all_to_all.25 = bf16[64,13,1024]{2,1,0:T(8,128)(2,1)} all-to-all(bf16[64,13,1024]{2,1,0:T(8,128)(2,1)S(1)} %constant_dynamic-slice_fusion), channel_id=1, replica_groups=mesh['grp'=2,'ep'=64,'tp'=2] {'ep'}, dimensions={0} | all-to-all | bytes 3407872 | tf_op jit(solution)/shard_map/all_to_all | solution.py:123
  168.5 1.6 fusion.67
  171.7 10.8 %all-gather.2.cloned.1.call-done = bf16[64,13,2048]{2,1,0:T(8,128)(2,1)} async-done(((bf16[64,13,1024]{2,1,0:T(8,128)(2,1)}), bf16[64,13,2048]{2,1,0:T(8,128)(2,1)}) %all-gather.2.cloned.1.call-update) | async-done | bytes 3407888 | tf_op jit(solution)/shard_map/all_gather | solution.py:122
  182.5 3.4 reshape.129
  185.9 2.4 fusion.8
  188.3 1.8 fusion.4
  191.3 2.3 convolution_convert_fusion
  194.1 6.5 %all_to_all.26 = bf16[2,64,13,1024]{3,1,2,0:T(8,128)(2,1)S(1)} all-to-all(bf16[2,64,13,1024]{3,1,2,0:T(8,128)(2,1)S(1)} %bitcast.84), channel_id=1, replica_groups=mesh['grp'=2,'ep'=64,'tp'=2] {'tp'}, dimensions={0} | all-to-all | bytes 6815744 | tf_op jit(solution)/shard_map/all_to_all | solution.py:27
  200.6 4.2 %all-to-all-start.4 = ((bf16[2,96,1024]{2,1,0:T(8,128)(2,1)}), bf16[2,96,1024]{2,1,0:T(8,128)(2,1)}, u32[]{:S(2)}, u32[]{:S(2)}) async-start(bf16[2,96,1024]{2,1,0:T(8,128)(2,1)} %bitcast.89), calls=%async_computation.4 | async-start | bytes 786432 | tf_op jit(solution)/shard_map/all_to_all | solution.py:27
  204.8 2.5 reduce_sum.66
  207.2 3.7 %copy.101 = bf16[64,13,1024]{2,1,0:T(8,128)(2,1)} copy(bf16[64,13,1024]{2,0,1:T(8,128)(2,1)} %reduce_sum.66) | data formatting | bytes 3407872 | tf_op jit(solution)/shard_map/reduce_sum | solution.py:28
  211.0 16.5 %all-to-all-start.3 = ((bf16[64,13,1024]{2,1,0:T(8,128)(2,1)}), bf16[64,13,1024]{2,1,0:T(8,128)(2,1)}, u32[]{:S(2)}, u32[]{:S(2)}) async-start(bf16[64,13,1024]{2,1,0:T(8,128)(2,1)} %copy.101), calls=%async_computation.3 | async-start | bytes 4194304 | tf_op jit(solution)/shard_map/all_to_all | solution.py:137
  228.8 1.8 convert_reduce_fusion.1
  231.9 95.9 %all-to-all-done.3 = bf16[64,13,1024]{2,1,0:T(8,128)(2,1)} async-done(((bf16[64,13,1024]{2,1,0:T(8,128)(2,1)}), bf16[64,13,1024]{2,1,0:T(8,128)(2,1)}, u32[]{:S(2)}, u32[]{:S(2)}) %all-to-all-start.3) | async-done | bytes 1703968 | tf_op jit(solution)/shard_map/all_to_all | solution.py:137
  327.8 2.6 reshape.131
  330.4 2.9 gather_fusion
  334.6 2.1 fusion.1
  (93 shorter events, 21.9 us)
Async XLA Ops:
  7.2 17.1 %copy-start = (bf16[512,2048]{1,0:T(8,128)(2,1)S(1)}, bf16[512,2048]{1,0:T(8,128)(2,1)}, u32[]{:S(2)}) copy-start(bf16[512,2048]{1,0:T(8,128)(2,1)} %param.30) | copy-start | bytes 6291460
  15.7 3.9 %copy-start.17 = (f32[32,64]{1,0:T(8,128)S(1)}, f32[32,64]{1,0:T(8,128)}, u32[]{:S(2)}) copy-start(f32[32,64]{1,0:T(8,128)} %param.25) | copy-start | bytes 24580
  15.7 3.9 %copy-start.18 = (f32[32,64]{1,0:T(8,128)S(1)}, f32[32,64]{1,0:T(8,128)}, u32[]{:S(2)}) copy-start(f32[32,64]{1,0:T(8,128)} %param.24) | copy-start | bytes 24580
  18.2 1.6 copy-start.9
  19.8 3.1 copy-start.14
  22.9 1.3 copy-start.4
  22.9 1.5 copy-start.20
  24.3 5.3 %copy-start.16 = (s32[96,6]{0,1:T(8,128)S(1)}, s32[96,6]{0,1:T(8,128)}, u32[]{:S(2)}) copy-start(s32[96,6]{0,1:T(8,128)} %param.38) | copy-start | bytes 6916
  25.8 6.8 %copy-start.10 = (bf16[96,2048]{1,0:T(8,128)(2,1)S(1)}, bf16[96,2048]{1,0:T(8,128)(2,1)}, u32[]{:S(2)}) copy-start(bf16[96,2048]{1,0:T(8,128)(2,1)} %param.20) | copy-start | bytes 1179652
  25.8 6.6 %all-to-all-start = ((bf16[2,96,2048]{2,1,0:T(8,128)(2,1)}), bf16[2,96,2048]{2,1,0:T(8,128)(2,1)S(1)}, u32[]{:S(2)}, u32[]{:S(2)}) async-start(bf16[2,96,2048]{2,1,0:T(8,128)(2,1)} %broadcast_in_dim.9), calls=%async_computation | async-start | bytes 1572864 | tf_op jit(solution)/shard_map/all_to_all | solution.py:11
  29.5 152.9 %all-gather.2.cloned.1.call-start = ((), (), s32[]{:S(2)}) async-start(), calls=%async_computation.5 | async-start | bytes 6291456 | tf_op jit(solution)/shard_map/all_gather | solution.py:122
  31.4 2.1 copy-start.15
  167.5 1.0 copy-start.7
  167.5 2.6 copy-start.12
  167.5 2.6 copy-start.13
  185.9 2.4 copy-start.21
  200.6 10.4 %all-to-all-start.4 = ((bf16[2,96,1024]{2,1,0:T(8,128)(2,1)}), bf16[2,96,1024]{2,1,0:T(8,128)(2,1)}, u32[]{:S(2)}, u32[]{:S(2)}) async-start(bf16[2,96,1024]{2,1,0:T(8,128)(2,1)} %bitcast.89), calls=%async_computation.4 | async-start | bytes 786432 | tf_op jit(solution)/shard_map/all_to_all | solution.py:27
  211.0 16.8 %copy-start.19 = (f32[96,6]{0,1:T(8,128)S(1)}, f32[96,6]{0,1:T(8,128)}, u32[]{:S(2)}) copy-start(f32[96,6]{0,1:T(8,128)} %param.39) | copy-start | bytes 6916
  211.0 17.1 %copy-start.5 = (f32[96,32,64]{0,2,1:T(8,128)S(1)}, f32[96,32,64]{0,2,1:T(8,128)}, u32[]{:S(2)}) copy-start(f32[96,32,64]{0,2,1:T(8,128)} %copy-done.4) | copy-start | bytes 2359300
  211.0 17.4 %copy-start.3 = (f32[96,32,64]{0,2,1:T(8,128)S(1)}, f32[96,32,64]{0,2,1:T(8,128)}, u32[]{:S(2)}) copy-start(f32[96,32,64]{0,2,1:T(8,128)} %copy-done.2) | copy-start | bytes 2359300
  211.0 116.8 %all-to-all-start.3 = ((bf16[64,13,1024]{2,1,0:T(8,128)(2,1)}), bf16[64,13,1024]{2,1,0:T(8,128)(2,1)}, u32[]{:S(2)}, u32[]{:S(2)}) async-start(bf16[64,13,1024]{2,1,0:T(8,128)(2,1)} %copy.101), calls=%async_computation.3 | async-start | bytes 4194304 | tf_op jit(solution)/shard_map/all_to_all | solution.py:137
  333.2 4.3 %copy-start.1 = (bf16[512,2048]{1,0:T(8,128)(2,1)S(1)}, bf16[512,2048]{1,0:T(8,128)(2,1)}, u32[]{:S(2)}) copy-start(bf16[512,2048]{1,0:T(8,128)(2,1)} %param.30) | copy-start | bytes 6291460
  334.6 2.1 copy-start.8
  334.6 2.1 copy-start.11
  (2 other events, 1.7 us)
Sparse Core Ops, SparseCore 0:
  167.7 14.7 all-gather.1
where the time goes:
time: 346 us; the launch traced here: 344 us
  blocking collectives  135 us (39%)
  waiting for transfers between devices  107 us (31%)
  local copies, waits for them, and re-layouts  34.1 us (10%)
  starting transfers between devices  24.5 us (7%)
  matrix products  19.7 us (6%)
  between operations  14.6 us (4%)
  other arithmetic  10.2 us (3%)
    all_to_all x1, blocking collectives, body(): lax.all_to_all(own_cols, 'ep', split_axis=0, concat_axis=0, tiled=True)  128 us
    all_to_all x1, waiting for transfers between devices, body(): lax.all_to_all(summed.astype(jnp.bfloat16), 'ep', split_axis=0, concat_ax...  95.9 us
    all_to_all x1, starting transfers between devices, body(): lax.all_to_all(summed.astype(jnp.bfloat16), 'ep', split_axis=0, concat_ax...  16.5 us
    all_gather x1, waiting for transfers between devices, body(): lax.all_gather(lax.all_to_all(own_cols, 'ep', split_axis=0, concat_axis=0...  10.8 us
  transfers between devices with their start and end apart: 4, of which 2 were waited for; matrix products, arithmetic and copies ran while one was open for 5% of the time, Pallas kernels for 0%

commit v1 on v0

--- a/solution.py
+++ b/solution.py
@@ -119,11 +119,17 @@
     outgoing = outgoing.reshape(experts, slot_cap, -1)
     half_cols = outgoing.shape[2] // lax.axis_size("tp")
     own_cols = lax.dynamic_slice_in_dim(outgoing, lax.axis_index("tp") * half_cols, half_cols, 2)
-    arrived = lax.all_gather(
-        lax.all_to_all(own_cols, "ep", split_axis=0, concat_axis=0, tiled=True),
-        "tp",
+    arrived = jnp.concatenate(
+        lax.all_to_all(
+            jnp.stack(
+                [lax.all_to_all(own_cols, "ep", split_axis=0, concat_axis=0, tiled=True)]
+                * lax.axis_size("tp")
+            ),
+            "tp",
+            0,
+            0,
+        ),
         axis=2,
-        tiled=True,
     )
     sources, count_items, full_width = arrived.shape
     expert_rows = arrived.reshape(sources * count_items, full_width)

time: 346 us -> 317 us (0.916)
  blocking collectives: 135 us -> 13 us
  waiting for transfers between devices: 107 us -> 192 us
  starting transfers between devices: 24.5 us -> 42.9 us
  between operations: 14.6 us -> 1.18 us
    all_to_all x1, blocking collectives: 128 us -> 6.49 us  [body(): lax.all_to_all(jnp.stack([lax.all_to_all(own_cols, 'ep', split_axis=0, co...]
    all_to_all x0 -> x1, waiting for transfers between devices: none -> 95.4 us  [body(): lax.all_to_all(own_cols, 'ep', split_axis=0, concat_axis=0, tiled=True)]
    all_to_all x0 -> x1, starting transfers between devices: none -> 28.2 us  [body(): lax.all_to_all(own_cols, 'ep', split_axis=0, concat_axis=0, tiled=True)]
    all_gather x1 -> x0, waiting for transfers between devices: 10.8 us -> none  [body(): lax.all_gather(lax.all_to_all(own_cols, 'ep', split_axis=0, concat_axis=0...]
    all_to_all x1, starting transfers between devices: 16.5 us -> 6.81 us  [body(): lax.all_to_all(summed.astype(jnp.bfloat16), 'ep', split_axis=0, concat_ax...]
  transfers between devices with their start and end apart: 4 -> 4, of which waited for: 2 -> 2; matrix products, arithmetic and copies ran while one was open for 5% -> 6% of each run, Pallas kernels for 0% -> 0%
where the time goes in v1:
time: 317 us; the launch traced here: 315 us
  waiting for transfers between devices  192 us (61%)
  starting transfers between devices  42.9 us (14%)
  local copies, waits for them, and re-layouts  37.1 us (12%)
  matrix products  18.1 us (6%)
  blocking collectives  13 us (4%)
  other arithmetic  11.5 us (4%)
    all_to_all x1, waiting for transfers between devices, body(): lax.all_to_all(summed.astype(jnp.bfloat16), 'ep', split_axis=0, concat_ax...  96.1 us
    all_to_all x1, waiting for transfers between devices, body(): lax.all_to_all(own_cols, 'ep', split_axis=0, concat_axis=0, tiled=True)  95.4 us
    all_to_all x1, starting transfers between devices, body(): lax.all_to_all(own_cols, 'ep', split_axis=0, concat_axis=0, tiled=True)  28.2 us
    all_to_all x1, starting transfers between devices, body(): lax.all_to_all(summed.astype(jnp.bfloat16), 'ep', split_axis=0, concat_ax...  6.81 us
    all_to_all x1, blocking collectives, body(): lax.all_to_all(jnp.stack([lax.all_to_all(own_cols, 'ep', split_axis=0, co...  6.49 us
    all_to_all x1, blocking collectives, summed_on_arrival(): lax.all_to_all(tiles, axis, split_axis=0, concat_axis=0, tiled=True)  6.49 us
  transfers between devices with their start and end apart: 4, of which 2 were waited for; matrix products, arithmetic and copies ran while one was open for 6% of the time, Pallas kernels for 0%

profile of v1, /device:TPU:34, one launch (start us, length us, event | category | flops | bytes accessed | tf_op | source)
XLA Modules:
  0.0 315.3 jit_solution(11936888106509632547)
XLA Ops:
  2.6 2.3 convolution_convert_fusion.4
  5.0 2.7 fusion.72
  9.2 2.5 copy.97
  13.3 3.0 bitcast_add_fusion
  19.3 3.7 %all-to-all-start = ((bf16[2,96,2048]{2,1,0:T(8,128)(2,1)}), bf16[2,96,2048]{2,1,0:T(8,128)(2,1)S(1)}, u32[]{:S(2)}, u32[]{:S(2)}) async-start(bf16[2,96,2048]{2,1,0:T(8,128)(2,1)} %broadcast_in_dim.9), calls=%async_computation | async-start | bytes 1572864 | tf_op jit(solution)/shard_map/all_to_all | solution.py:11
  28.6 2.9 reshape.128
  31.5 3.2 %constant_dynamic-slice_fusion = bf16[64,13,1024]{2,1,0:T(8,128)(2,1)} fusion(bf16[64,13,2048]{2,1,0:T(8,128)(2,1)} %reshape.128, s32[]{:T(128)S(6)} %select_n.26), kind=kLoop, calls=%fused_computation.101 | loop fusion | bytes 3407876 | tf_op jit(solution)/shard_map/dynamic_slice | solution.py:121
  34.8 28.2 %all-to-all-start.1 = ((bf16[64,13,1024]{2,1,0:T(8,128)(2,1)}), bf16[64,13,1024]{2,1,0:T(8,128)(2,1)S(1)}, u32[]{:S(2)}, u32[]{:S(2)}) async-start(bf16[64,13,1024]{2,1,0:T(8,128)(2,1)} %constant_dynamic-slice_fusion), calls=%async_computation.1 | async-start | bytes 4194304 | tf_op jit(solution)/shard_map/all_to_all | solution.py:125
  63.0 1.6 fusion.67
  64.7 2.4 convolution_convert_fusion.2
  67.8 95.4 %all-to-all-done.1 = bf16[64,13,1024]{2,1,0:T(8,128)(2,1)S(1)} async-done(((bf16[64,13,1024]{2,1,0:T(8,128)(2,1)}), bf16[64,13,1024]{2,1,0:T(8,128)(2,1)S(1)}, u32[]{:S(2)}, u32[]{:S(2)}) %all-to-all-start.1) | async-done | bytes 1703968 | tf_op jit(solution)/shard_map/all_to_all | solution.py:125
  164.0 2.0 copy.105
  166.0 6.5 %all_to_all.30 = bf16[2,64,13,1024]{3,1,2,0:T(8,128)(2,1)S(1)} all-to-all(bf16[2,64,13,1024]{3,1,2,0:T(8,128)(2,1)S(1)} %copy.105), channel_id=1, replica_groups=mesh['grp'=2,'ep'=64,'tp'=2] {'tp'}, dimensions={0} | all-to-all | bytes 6815744 | tf_op jit(solution)/shard_map/all_to_all | solution.py:123
  172.5 3.5 %copy.106 = bf16[64,13,2,1024]{3,2,1,0:T(2,128)(2,1)S(1)} copy(bf16[64,13,2,1024]{3,0,1,2:T(8,128)(2,1)S(1)} %bitcast.89) | data formatting | bytes 6815744 | tf_op jit(solution)/shard_map/reshape | solution.py:122
  181.3 6.5 %all_to_all.31 = bf16[2,64,13,1024]{3,1,2,0:T(8,128)(2,1)S(1)} all-to-all(bf16[2,64,13,1024]{3,1,2,0:T(8,128)(2,1)S(1)} %bitcast.91), channel_id=1, replica_groups=mesh['grp'=2,'ep'=64,'tp'=2] {'tp'}, dimensions={0} | all-to-all | bytes 6815744 | tf_op jit(solution)/shard_map/all_to_all | solution.py:27
  187.8 4.2 %all-to-all-start.5 = ((bf16[2,96,1024]{2,1,0:T(8,128)(2,1)}), bf16[2,96,1024]{2,1,0:T(8,128)(2,1)}, u32[]{:S(2)}, u32[]{:S(2)}) async-start(bf16[2,96,1024]{2,1,0:T(8,128)(2,1)} %bitcast.99), calls=%async_computation.5 | async-start | bytes 786432 | tf_op jit(solution)/shard_map/all_to_all | solution.py:27
  191.9 2.5 reduce_sum.66
  194.4 3.7 %copy.110 = bf16[64,13,1024]{2,1,0:T(8,128)(2,1)} copy(bf16[64,13,1024]{2,0,1:T(8,128)(2,1)} %reduce_sum.66) | data formatting | bytes 3407872 | tf_op jit(solution)/shard_map/reduce_sum | solution.py:28
  198.2 6.8 %all-to-all-start.4 = ((bf16[64,13,1024]{2,1,0:T(8,128)(2,1)}), bf16[64,13,1024]{2,1,0:T(8,128)(2,1)}, u32[]{:S(2)}, u32[]{:S(2)}) async-start(bf16[64,13,1024]{2,1,0:T(8,128)(2,1)} %copy.110), calls=%async_computation.4 | async-start | bytes 4194304 | tf_op jit(solution)/shard_map/all_to_all | solution.py:143
  206.3 1.8 convert_reduce_fusion.1
  209.4 96.1 %all-to-all-done.4 = bf16[64,13,1024]{2,1,0:T(8,128)(2,1)} async-done(((bf16[64,13,1024]{2,1,0:T(8,128)(2,1)}), bf16[64,13,1024]{2,1,0:T(8,128)(2,1)}, u32[]{:S(2)}, u32[]{:S(2)}) %all-to-all-start.4) | async-done | bytes 1703968 | tf_op jit(solution)/shard_map/all_to_all | solution.py:143
  305.5 2.6 reshape.131
  308.1 2.9 gather_fusion
  312.4 2.1 fusion.1
  (101 shorter events, 25.0 us)
Async XLA Ops:
  0.6 17.2 %copy-start = (bf16[512,2048]{1,0:T(8,128)(2,1)S(1)}, bf16[512,2048]{1,0:T(8,128)(2,1)}, u32[]{:S(2)}) copy-start(bf16[512,2048]{1,0:T(8,128)(2,1)} %param.30) | copy-start | bytes 6291460
  9.2 3.9 %copy-start.17 = (f32[32,64]{1,0:T(8,128)S(1)}, f32[32,64]{1,0:T(8,128)}, u32[]{:S(2)}) copy-start(f32[32,64]{1,0:T(8,128)} %param.25) | copy-start | bytes 24580
  9.2 3.9 %copy-start.18 = (f32[32,64]{1,0:T(8,128)S(1)}, f32[32,64]{1,0:T(8,128)}, u32[]{:S(2)}) copy-start(f32[32,64]{1,0:T(8,128)} %param.24) | copy-start | bytes 24580
  11.7 1.6 copy-start.9
  13.3 3.1 copy-start.14
  16.3 1.3 copy-start.4
  16.3 1.5 copy-start.22
  17.8 5.2 %copy-start.16 = (s32[96,6]{0,1:T(8,128)S(1)}, s32[96,6]{0,1:T(8,128)}, u32[]{:S(2)}) copy-start(s32[96,6]{0,1:T(8,128)} %param.38) | copy-start | bytes 6916
  19.3 7.2 %copy-start.10 = (bf16[96,2048]{1,0:T(8,128)(2,1)S(1)}, bf16[96,2048]{1,0:T(8,128)(2,1)}, u32[]{:S(2)}) copy-start(bf16[96,2048]{1,0:T(8,128)(2,1)} %param.20) | copy-start | bytes 1179652
  19.3 7.1 %all-to-all-start = ((bf16[2,96,2048]{2,1,0:T(8,128)(2,1)}), bf16[2,96,2048]{2,1,0:T(8,128)(2,1)S(1)}, u32[]{:S(2)}, u32[]{:S(2)}) async-start(bf16[2,96,2048]{2,1,0:T(8,128)(2,1)} %broadcast_in_dim.9), calls=%async_computation | async-start | bytes 1572864 | tf_op jit(solution)/shard_map/all_to_all | solution.py:11
  24.8 2.7 copy-start.15
  26.8 4.8 %copy-start.19 = (f32[96]{0:T(128)}, f32[96]{0:T(128)S(1)}, u32[]{:S(2)}) copy-start(f32[96]{0:T(128)S(1)} %add_rsqrt_fusion) | copy-start | bytes 1156
  34.8 28.3 %copy-start.7 = (bf16[96,2048]{1,0:T(8,128)(2,1)S(1)}, bf16[96,2048]{1,0:T(8,128)(2,1)}, u32[]{:S(2)}) copy-start(bf16[96,2048]{1,0:T(8,128)(2,1)} %copy-done.6) | copy-start | bytes 1179652
  34.8 28.3 %copy-start.13 = (bf16[2048,256]{1,0:T(8,128)(2,1)S(1)}, bf16[2048,256]{1,0:T(8,128)(2,1)}, u32[]{:S(2)}) copy-start(bf16[2048,256]{1,0:T(8,128)(2,1)} %param.35) | copy-start | bytes 3145732
  34.8 128.4 %all-to-all-start.1 = ((bf16[64,13,1024]{2,1,0:T(8,128)(2,1)}), bf16[64,13,1024]{2,1,0:T(8,128)(2,1)S(1)}, u32[]{:S(2)}, u32[]{:S(2)}) async-start(bf16[64,13,1024]{2,1,0:T(8,128)(2,1)} %constant_dynamic-slice_fusion), calls=%async_computation.1 | async-start | bytes 4194304 | tf_op jit(solution)/shard_map/all_to_all | solution.py:125
  187.8 10.4 %all-to-all-start.5 = ((bf16[2,96,1024]{2,1,0:T(8,128)(2,1)}), bf16[2,96,1024]{2,1,0:T(8,128)(2,1)}, u32[]{:S(2)}, u32[]{:S(2)}) async-start(bf16[2,96,1024]{2,1,0:T(8,128)(2,1)} %bitcast.99), calls=%async_computation.5 | async-start | bytes 786432 | tf_op jit(solution)/shard_map/all_to_all | solution.py:27
  198.2 7.1 %copy-start.20 = (f32[96,6]{0,1:T(8,128)S(1)}, f32[96,6]{0,1:T(8,128)}, u32[]{:S(2)}) copy-start(f32[96,6]{0,1:T(8,128)} %param.39) | copy-start | bytes 6916
  198.2 7.3 %copy-start.21 = (pred[96,6]{0,1:T(8,128)(4,1)S(1)}, pred[96,6]{0,1:T(8,128)(4,1)}, u32[]{:S(2)}) copy-start(pred[96,6]{0,1:T(8,128)(4,1)} %get-tuple-element.2) | copy-start | bytes 1732
  198.2 7.4 %copy-start.5 = (f32[96,32,64]{0,2,1:T(8,128)S(1)}, f32[96,32,64]{0,2,1:T(8,128)}, u32[]{:S(2)}) copy-start(f32[96,32,64]{0,2,1:T(8,128)} %copy-done.4) | copy-start | bytes 2359300
  198.2 7.7 %copy-start.3 = (f32[96,32,64]{0,2,1:T(8,128)S(1)}, f32[96,32,64]{0,2,1:T(8,128)}, u32[]{:S(2)}) copy-start(f32[96,32,64]{0,2,1:T(8,128)} %copy-done.2) | copy-start | bytes 2359300
  198.2 107.3 %all-to-all-start.4 = ((bf16[64,13,1024]{2,1,0:T(8,128)(2,1)}), bf16[64,13,1024]{2,1,0:T(8,128)(2,1)}, u32[]{:S(2)}, u32[]{:S(2)}) async-start(bf16[64,13,1024]{2,1,0:T(8,128)(2,1)} %copy.110), calls=%async_computation.4 | async-start | bytes 4194304 | tf_op jit(solution)/shard_map/all_to_all | solution.py:143
  311.0 4.3 %copy-start.1 = (bf16[512,2048]{1,0:T(8,128)(2,1)S(1)}, bf16[512,2048]{1,0:T(8,128)(2,1)}, u32[]{:S(2)}) copy-start(bf16[512,2048]{1,0:T(8,128)(2,1)} %param.30) | copy-start | bytes 6291460
  312.4 2.1 copy-start.8
  312.4 2.1 copy-start.11
  (5 other events, 5.4 us)
